TPU v7x, 256 devices: a whole 4x4x8 slice. The times are simulated.
256 devices in a mesh: sp: 32 (over z, y), dp: 8 (over x, core).
Axes of the slice: x: 4, y: 4, z: 8, core: 2. Of those that a mesh axis runs over, the one named last changes fastest.
Arguments:
- queries: bfloat16 [32, 16, 2048, 128], P('dp', None, 'sp'), may hold values from -6 to 6
- key_maps: bfloat16 [32, 16, 2048, 128], P('dp', None, 'sp'), may hold values from -6 to 6
- value_rows: bfloat16 [32, 16, 2048, 128], P('dp', None, 'sp'), may hold values from -6 to 6
- gate_logits: bfloat16 [2048, 32, 2048], P('sp', 'dp'), may hold values from -6 to 6
- mix_lambda: float32 [16], replicated, may hold values from 0.3 to 0.8
- head_gain: float32 [128], replicated, may hold values from 0.1 to 1.9
- out_weight: bfloat16 [2048, 2048], P('sp', 'dp'), may hold values from -0.125 to 0.125
Outputs:
- projected: bfloat16 [2048, 32, 2048], P('sp', 'dp')
All inputs are finite; a program needn't handle non-finite values.
Results may differ from a plain program's by a relative error of at most 0.0075.
Values may be sent and summed in bfloat16 or wider, within the bound.
A program may use at most 64 MiB of HBM per device.

v0:
```python
import jax
import jax.numpy as jnp
from jax import lax
from jax.sharding import Mesh
from jax.sharding import PartitionSpec as P

HEAD_DIM = 64
STRETCH = 64
BLOCK = 512
SP = ("sp_0", "sp_1")


def side_by_side(arrays, axis, split_dim, concat_dim, along):
    ends, at = ([], 0)
    for a in arrays[:-1]:
        at += a.shape[along]
        ends.append(at)
    both = jnp.concatenate(arrays, axis=along)
    return tuple(
        jnp.split(
            lax.all_to_all(both, axis, split_axis=split_dim, concat_axis=concat_dim, tiled=True),
            ends,
            axis=along,
        )
    )


def shortened(shard):
    return jax.tree.map(lambda a: a.astype(jnp.bfloat16) if a.dtype == jnp.float32 else a, shard)


def gather_axes(shard, axes, dim):
    out = shard
    for number in range(len(axes) - 1, -1, -1):
        out = lax.all_gather(out, axes[number], axis=dim, tiled=True)
    return out


def attend(operands, head_gain):
    query_item, key_item, value_item, weight_two = operands
    length = query_item.shape[0]
    half_cols = query_item.shape[1] // 2
    value_cols = value_item.shape[1]
    block_len = min(BLOCK, length)
    n_blocks = length // block_len
    score_scale = HEAD_DIM ** (-0.5)
    in_segment = jnp.arange(block_len) // STRETCH
    diag_visible = in_segment[None, :] <= in_segment[:, None]

    def query_block(block_index):
        offset = block_index * block_len
        query_rows = lax.dynamic_slice_in_dim(query_item, offset, block_len, 0)

        def update(carry_state, key_block, value_block, visible):
            updated = []
            for which in range(2):
                running, summed, carried = carry_state[which]
                scores = (
                    jnp.dot(
                        query_rows[:, which * half_cols : (which + 1) * half_cols],
                        key_block[:, which * half_cols : (which + 1) * half_cols].T,
                        preferred_element_type=jnp.float32,
                    )
                    * score_scale
                )
                if visible is not None:
                    scores = jnp.where(visible, scores, -1e30)
                highest = jnp.maximum(running, jnp.max(scores, axis=1, keepdims=True))
                rescale = jnp.exp(running - highest)
                weights = jnp.exp(scores - highest)
                summed = summed * rescale + jnp.sum(weights, axis=1, keepdims=True)
                carried = carried * rescale + jnp.dot(
                    weights.astype(jnp.bfloat16), value_block, preferred_element_type=jnp.float32
                )
                updated.append((highest, summed, carried))
            return tuple(updated)

        def advance(key_index, carry_state):
            key_block = lax.dynamic_slice_in_dim(key_item, key_index * block_len, block_len, 0)
            value_block = lax.dynamic_slice_in_dim(value_item, key_index * block_len, block_len, 0)
            return update(carry_state, key_block, value_block, None)

        initial = tuple(
            (
                (
                    jnp.full((block_len, 1), -1e30, jnp.float32),
                    jnp.zeros((block_len, 1), jnp.float32),
                    jnp.zeros((block_len, value_cols), jnp.float32),
                )
                for which in range(2)
            )
        )
        carry_state = lax.fori_loop(0, block_index, advance, initial)
        carry_state = update(
            carry_state,
            lax.dynamic_slice_in_dim(key_item, offset, block_len, 0),
            lax.dynamic_slice_in_dim(value_item, offset, block_len, 0),
            diag_visible,
        )
        combined = carry_state[0][2] / carry_state[0][1] - weight_two * (
            carry_state[1][2] / carry_state[1][1]
        )
        mean_sq = jnp.mean(combined * combined, axis=1, keepdims=True)
        return (combined * lax.rsqrt(mean_sq + 1e-05) * head_gain).astype(jnp.bfloat16)

    pieces = lax.map(query_block, jnp.arange(n_blocks))
    return pieces.reshape(length, value_cols)


def on_device(queries, key_maps, value_rows, gate_logits, mix_lambda, head_gain, out_weight):
    seq_count, head_count, tok_rows, q_cols = queries.shape
    value_cols = value_rows.shape[3]
    item_count = seq_count * head_count
    model_width = gate_logits.shape[2]
    moved = side_by_side(
        (
            queries.reshape(item_count, tok_rows, q_cols),
            key_maps.reshape(item_count, tok_rows, q_cols),
            value_rows.reshape(item_count, tok_rows, value_cols),
        ),
        SP,
        0,
        1,
        2,
    )
    query_all, key_all, value_all = moved
    per_dev = query_all.shape[0]
    first_item = lax.axis_index(SP) * per_dev
    head_ids = (first_item + jnp.arange(per_dev)) % head_count
    matches = head_ids[:, None] == jnp.arange(head_count)[None, :]
    lambda_local = jnp.sum(jnp.where(matches, mix_lambda[None, :], 0.0), axis=1)

    def attend_one(operands):
        return attend(operands, head_gain)

    normed = lax.map(attend_one, (query_all, key_all, value_all, lambda_local))
    returned = lax.all_to_all(
        shortened(jnp.swapaxes(normed, 0, 1)), SP, split_axis=0, concat_axis=1, tiled=True
    )
    by_token = returned.reshape(tok_rows, seq_count, model_width)
    gated = (jax.nn.sigmoid(gate_logits.astype(jnp.float32)) * by_token.astype(jnp.float32)).astype(
        jnp.bfloat16
    )
    gated_rows = gated.reshape(tok_rows * seq_count, model_width)
    gathered = gather_axes(out_weight, SP, 0)
    result = jnp.dot(
        gated_rows,
        lax.all_gather(gathered, "dp", axis=1, tiled=True),
        preferred_element_type=jnp.float32,
    )
    return result.astype(jnp.bfloat16).reshape(tok_rows, seq_count, model_width)


def solution(mesh):
    torus = Mesh(mesh.devices.reshape(8, 4, mesh.shape["dp"]), ("sp_0", "sp_1", "dp"))
    return jax.shard_map(
        on_device,
        mesh=torus,
        in_specs=(
            P("dp", None, SP, None),
            P("dp", None, SP, None),
            P("dp", None, SP, None),
            P(SP, "dp", None),
            P(),
            P(),
            P(SP, "dp"),
        ),
        out_specs=P(SP, "dp", None),
        check_vma=False,
    )
```

profile of v0, /device:TPU:64, one launch (start us, length us, event | category | flops | bytes accessed | tf_op | source)
XLA Modules:
  0.0 283.0 jit_solution(14072535416872751660)
XLA Ops:
  6.5 4.1 %pad_maximum_fusion = bf16[64,64,384]{2,1,0:T(8,128)(2,1)} fusion(bf16[64,64,128]{2,1,0:T(8,128)(2,1)} %bitcast.122, bf16[64,64,128]{2,1,0:T(8,128)(2,1)} %bitcast.123, bf16[64,64,128]{2,1,0:T(8,128)(2,1)} %bitcast.124), kind=kLoop, calls=%fused_computation.74 | loop fusion | flops 9437184 | bytes 6291456 | tf_op jit(solution)/shard_map/concatenate | solution.py:18
  10.6 11.0 %all-to-all-start = ((bf16[64,64,384]{2,1,0:T(8,128)(2,1)}), bf16[64,64,384]{2,1,0:T(8,128)(2,1)S(1)}, u32[]{:S(2)}, u32[]{:S(2)}) async-start(bf16[64,64,384]{2,1,0:T(8,128)(2,1)} %pad_maximum_fusion), calls=%async_computation | async-start | bytes 6291456 | tf_op jit(solution)/shard_map/all_to_all | solution.py:21
  21.7 17.7 %all_gather.9 = bf16[256,256]{1,0:T(8,128)(2,1)} all-gather(bf16[64,256]{1,0:T(8,128)(2,1)S(1)} %copy-done.3), channel_id=1, replica_groups=mesh['sp_0'=8,'sp_1'=4,'dp'=8] {'sp_1'}, dimensions={0}, use_global_device_ids=true | all-gather | bytes 163840 | tf_op jit(solution)/shard_map/all_gather | solution.py:35
  39.7 56.3 %all-gather.3.cloned.1.call-done = bf16[2048,256]{1,0:T(8,128)(2,1)} async-done(((bf16[256,256]{1,0:T(8,128)(2,1)}), bf16[2048,256]{1,0:T(8,128)(2,1)}) %all-gather.3.cloned.1.call-update) | async-done | bytes 1048592 | tf_op jit(solution)/shard_map/all_gather | solution.py:35
  96.1 5.7 %all-to-all-done = bf16[64,64,384]{2,1,0:T(8,128)(2,1)S(1)} async-done(((bf16[64,64,384]{2,1,0:T(8,128)(2,1)}), bf16[64,64,384]{2,1,0:T(8,128)(2,1)S(1)}, u32[]{:S(2)}, u32[]{:S(2)}) %all-to-all-start) | async-done | bytes 3145760 | tf_op jit(solution)/shard_map/all_to_all | solution.py:21
  102.1 2.0 fusion.53
  104.1 118.3 %while.57 = (s32[]{:T(128)}, bf16[2,2048,128]{2,1,0:T(8,128)(2,1)}, bf16[2,2048,128]{2,1,0:T(8,128)(2,1)}, bf16[2,2048,128]{2,1,0:T(8,128)(2,1)}, bf16[2,2048,12...) while((s32[]{:T(128)}, bf16[2,2048,128]{2,1,0:T(8,128)(2,1)}, ...), condition=%wide.region_15.16_spmd, body=%wide.region_1.15_spmd.sunk | while | flops 411116032 | bytes 27815496 | solution.py:136
  104.1 1.3 dynamic-slice_bitcast_fusion.6
  105.3 1.1 dynamic-slice_bitcast_fusion.5
  107.1 54.3 %while.58 = (s32[]{:T(128)}, bf16[4,512,128]{2,1,0:T(8,128)(2,1)}, s32[4]{0:T(128)S(1)}, bf16[2048,128]{1,0:T(8,128)(2,1)S(1)}, bf16[2048,128]{1,0:T(8,128)(2,1)...) while((s32[]{:T(128)}, bf16[4,512,128]{2,1,0:T(8,128)(2,1)}, ...), condition=%wide.region_14.14_spmd.clone.clone, body=%wide.region_2.13_spmd.clone.clone.sunk | while | flops 411111936 | bytes 23618224 | solution.py:106
  110.1 1.0 copy-done
  111.5 2.3 fusion.78
  113.8 2.0 multiply_reduce_fusion.2
  118.1 3.3 %while.59 = (s32[]{:T(128)}, f32[512,1]{0,1:T(1,128)S(1)}, f32[512,1]{0,1:T(1,128)S(1)}, f32[512,128]{1,0:T(8,128)S(1)}, f32[512,1]{0,1:T(1,128)S(1)}, /*index=5...) while((s32[]{:T(128)}, f32[512,1]{0,1:T(1,128)S(1)}, ...), condition=%wide.region_8.7_spmd, body=%wide.region_3.6_spmd.sunk | while | flops 204736512 | bytes 8192227 | solution.py:93
  123.7 2.3 fusion.78
  126.1 2.0 multiply_reduce_fusion.2
  130.4 5.9 %while.59 = (s32[]{:T(128)}, f32[512,1]{0,1:T(1,128)S(1)}, f32[512,1]{0,1:T(1,128)S(1)}, f32[512,128]{1,0:T(8,128)S(1)}, f32[512,1]{0,1:T(1,128)S(1)}, /*index=5...) while((s32[]{:T(128)}, f32[512,1]{0,1:T(1,128)S(1)}, ...), condition=%wide.region_8.7_spmd, body=%wide.region_3.6_spmd.sunk | while | flops 204736512 | bytes 8192227 | solution.py:93
  138.6 2.3 fusion.78
  141.0 2.0 multiply_reduce_fusion.2
  145.3 8.5 %while.59 = (s32[]{:T(128)}, f32[512,1]{0,1:T(1,128)S(1)}, f32[512,1]{0,1:T(1,128)S(1)}, f32[512,128]{1,0:T(8,128)S(1)}, f32[512,1]{0,1:T(1,128)S(1)}, /*index=5...) while((s32[]{:T(128)}, f32[512,1]{0,1:T(1,128)S(1)}, ...), condition=%wide.region_8.7_spmd, body=%wide.region_3.6_spmd.sunk | while | flops 204736512 | bytes 8192227 | solution.py:93
  156.1 2.3 fusion.78
  158.5 2.0 multiply_reduce_fusion.2
  161.4 1.9 bitcast_dynamic-update-slice_fusion.2
  163.3 1.3 dynamic-slice_bitcast_fusion.6
  164.5 1.1 dynamic-slice_bitcast_fusion.5
  166.3 54.3 %while.58 = (s32[]{:T(128)}, bf16[4,512,128]{2,1,0:T(8,128)(2,1)}, s32[4]{0:T(128)S(1)}, bf16[2048,128]{1,0:T(8,128)(2,1)S(1)}, bf16[2048,128]{1,0:T(8,128)(2,1)...) while((s32[]{:T(128)}, bf16[4,512,128]{2,1,0:T(8,128)(2,1)}, ...), condition=%wide.region_14.14_spmd.clone.clone, body=%wide.region_2.13_spmd.clone.clone.sunk | while | flops 411111936 | bytes 23618224 | solution.py:106
  169.3 1.0 copy-done
  170.7 2.3 fusion.78
  173.0 2.0 multiply_reduce_fusion.2
  177.3 3.3 %while.59 = (s32[]{:T(128)}, f32[512,1]{0,1:T(1,128)S(1)}, f32[512,1]{0,1:T(1,128)S(1)}, f32[512,128]{1,0:T(8,128)S(1)}, f32[512,1]{0,1:T(1,128)S(1)}, /*index=5...) while((s32[]{:T(128)}, f32[512,1]{0,1:T(1,128)S(1)}, ...), condition=%wide.region_8.7_spmd, body=%wide.region_3.6_spmd.sunk | while | flops 204736512 | bytes 8192227 | solution.py:93
  181.5 1.0 copy-done
  182.9 2.3 fusion.78
  185.3 2.0 multiply_reduce_fusion.2
  189.6 5.9 %while.59 = (s32[]{:T(128)}, f32[512,1]{0,1:T(1,128)S(1)}, f32[512,1]{0,1:T(1,128)S(1)}, f32[512,128]{1,0:T(8,128)S(1)}, f32[512,1]{0,1:T(1,128)S(1)}, /*index=5...) while((s32[]{:T(128)}, f32[512,1]{0,1:T(1,128)S(1)}, ...), condition=%wide.region_8.7_spmd, body=%wide.region_3.6_spmd.sunk | while | flops 204736512 | bytes 8192227 | solution.py:93
  196.4 1.0 copy-done
  197.8 2.3 fusion.78
  200.2 2.0 multiply_reduce_fusion.2
  204.4 8.5 %while.59 = (s32[]{:T(128)}, f32[512,1]{0,1:T(1,128)S(1)}, f32[512,1]{0,1:T(1,128)S(1)}, f32[512,128]{1,0:T(8,128)S(1)}, f32[512,1]{0,1:T(1,128)S(1)}, /*index=5...) while((s32[]{:T(128)}, f32[512,1]{0,1:T(1,128)S(1)}, ...), condition=%wide.region_8.7_spmd, body=%wide.region_3.6_spmd.sunk | while | flops 204736512 | bytes 8192227 | solution.py:93
  215.3 2.3 fusion.78
  217.7 2.0 multiply_reduce_fusion.2
  220.5 1.9 bitcast_dynamic-update-slice_fusion.2
  222.4 2.8 %copy.36 = bf16[2,2048,128]{2,0,1:T(2,128)(2,1)S(1)} copy(bf16[2,2048,128]{2,1,0:T(8,128)(2,1)} %get-tuple-element.794) | data formatting | bytes 2097152 | tf_op jit(solution)/shard_map/while | solution.py:136
  225.3 35.8 %all_to_all.27 = bf16[2048,2,128]{2,1,0:T(2,128)(2,1)S(1)} all-to-all(bf16[2048,2,128]{2,1,0:T(2,128)(2,1)S(1)} %bitcast.115), channel_id=1, replica_groups=mesh['sp_0'=8,'sp_1'=4,'dp'=8] {'sp_0','sp_1'}, dimensions={0} | all-to-all | bytes 2097152 | tf_op jit(solution)/shard_map/all_to_all | solution.py:137
  262.0 1.2 copy.32
  263.2 3.0 %reshape.79 = f32[64,4,2048]{2,1,0:T(4,128)} reshape(f32[64,32,2,128]{3,2,1,0:T(2,128)S(1)} %copy.32) | data formatting | bytes 4194304 | tf_op jit(solution)/shard_map/convert_element_type | solution.py:141
  266.2 2.7 fusion.46
  269.2 5.7 %convolution_convert_fusion = bf16[256,2048]{1,0:T(8,128)(2,1)S(1)} fusion(bf16[256,2048]{1,0:T(8,128)(2,1)S(1)} %reshape.77, bf16[2048,2048]{1,0:T(8,128)(2,1)} %all-gather.5.cloned.1.call-done), kind=kOutput, calls=%fused_computation.75 | convolution fusion | flops 2148007936 | bytes 10485760 | tf_op jit(solution)/shard_map/dot_general | solution.py:146
  274.9 1.2 reshape.78
  (341 shorter events, 55.4 us)
Async XLA Ops:
  10.6 11.1 %copy-start.3 = (bf16[64,256]{1,0:T(8,128)(2,1)S(1)}, bf16[64,256]{1,0:T(8,128)(2,1)}, u32[]{:S(2)}) copy-start(bf16[64,256]{1,0:T(8,128)(2,1)} %param.19) | copy-start | bytes 98308
  10.6 28.9 %copy-start.4 = (f32[16]{0:T(128)S(1)}, f32[16]{0:T(128)}, u32[]{:S(2)}) copy-start(f32[16]{0:T(128)} %param.17) | copy-start | bytes 196
  10.6 91.1 %all-to-all-start = ((bf16[64,64,384]{2,1,0:T(8,128)(2,1)}), bf16[64,64,384]{2,1,0:T(8,128)(2,1)S(1)}, u32[]{:S(2)}, u32[]{:S(2)}) async-start(bf16[64,64,384]{2,1,0:T(8,128)(2,1)} %pad_maximum_fusion), calls=%async_computation | async-start | bytes 6291456 | tf_op jit(solution)/shard_map/all_to_all | solution.py:21
  21.7 74.3 %all-gather.3.cloned.1.call-start = ((), (), s32[]{:S(2)}) async-start(), calls=%async_computation.2 | async-start | bytes 1179648 | tf_op jit(solution)/shard_map/all_gather | solution.py:35
  39.4 229.8 %all-gather.5.cloned.1.call-start = ((), (), s32[]{:S(2)}) async-start(), calls=%async_computation.3 | async-start | bytes 9437184 | tf_op jit(solution)/shard_map/all_gather | solution.py:148
  102.1 2.0 copy-start.2
  110.1 1.1 copy-start
  122.3 1.1 copy-start
  137.2 1.1 copy-start
  154.7 1.1 copy-start
  169.2 1.1 copy-start
  181.5 1.1 copy-start
  196.4 1.1 copy-start
  213.9 1.1 copy-start
  263.2 3.1 %copy-start.1 = (bf16[64,4,2048]{2,1,0:T(4,128)(2,1)S(1)}, bf16[64,4,2048]{2,1,0:T(4,128)(2,1)}, u32[]{:S(2)}) copy-start(bf16[64,4,2048]{2,1,0:T(4,128)(2,1)} %param.16) | copy-start | bytes 3145732
Sparse Core Ops, SparseCore 0:
  39.6 56.4 all-gather.2
  97.9 61.2 all-gather.4
where the time goes:
time: 285 us; the launch traced here: 283 us
  matrix products  63.3 us (22%)
  waiting for transfers between devices  62 us (22%)
  blocking collectives  53.5 us (19%)
  local copies, waits for them, and re-layouts  42.6 us (15%)
  loops' own time  19.8 us (7%)
  other arithmetic  17.1 us (6%)
  between operations  13.5 us (5%)
  starting transfers between devices  11.1 us (4%)
    all_gather x1, waiting for transfers between devices, gather_axes(): out = lax.all_gather(out, axes[number], axis=dim, tiled=True)  56.3 us
    dot_general x40, matrix products, update(): jnp.dot(weights.astype(jnp.bfloat16), value_block, preferred_element_type...  43.4 us
    all_to_all x1, blocking collectives, on_device(): lax.all_to_all(shortened(jnp.swapaxes(normed, 0, 1)), SP, split_axis=0, c...  35.8 us
    all_gather x1, blocking collectives, gather_axes(): out = lax.all_gather(out, axes[number], axis=dim, tiled=True)  17.7 us
    dot_general x40, matrix products, update(): jnp.dot(query_rows[:, which * half_cols:(which + 1) * half_cols], key_blo...  14.2 us
    another operation x8, loops' own time, query_block(): carry_state = lax.fori_loop(0, block_index, advance, initial)  13.5 us
    all_to_all x1, starting transfers between devices, side_by_side(): lax.all_to_all(both, axis, split_axis=split_dim, concat_axis=concat_dim,...  11 us
    while x40, local copies, waits for them, and re-layouts  8.32 us
  transfers between devices with their start and end apart: 3, of which 2 were waited for; matrix products, arithmetic and copies ran while one was open for 37% of the time, Pallas kernels for 0%

commit v1 on v0

v1 whole, which is shorter than its diff:
```python
import functools
import math

import jax
import jax.numpy as jnp
from jax import lax
from jax.experimental import pallas as pl
from jax.experimental.pallas import tpu as pltpu
from jax.sharding import PartitionSpec as P

MESH = pl.DeviceIdType.MESH
HEAD_DIM = 64
NZ, NY, NX = 8, 4, 4
NSP, NDP = NZ * NY, 2 * NX
EXP_SCALE = HEAD_DIM ** (-0.5) * math.log2(math.e)
F32, BF16 = jnp.float32, jnp.bfloat16


def slab_offset(step):
    half = (step + 1) // 2
    return jnp.where(step % 2 == 1, half, lax.rem(NZ - half, NZ))


def slab_attention(s, item, recv, vt, scores, ostage, lam, gain):
    lane = lax.broadcasted_iota(jnp.int32, (128, 128), 1)
    half_lane = lax.rem(lax.broadcasted_iota(jnp.int32, (64, 256), 1), 128)
    for h in range(2):
        first = NY * s + 2 * h
        q = recv[item, pl.ds(first, 2), 2].reshape(128, 128)
        zero = jnp.zeros_like(q)
        qm = jnp.concatenate(
            [jnp.where(lane < HEAD_DIM, q, zero), jnp.where(lane >= HEAD_DIM, q, zero)], axis=0
        )
        chunks = first + 2
        blocks = []
        at = 0
        while at < chunks:
            size = min(4, chunks - at)
            blocks.append((at, size))
            at += size
        highest = jnp.full((8, 256), -1e30, F32)
        for at, size in blocks:
            rows = 64 * size
            keys = recv[item, pl.ds(at, size), 0].reshape(rows, 128)
            st = lax.dot_general(
                keys, qm, (((1,), (1,)), ((), ())), preferred_element_type=F32
            )
            if at + size == chunks:
                tail = jnp.where(half_lane < 64, -1e30, st[rows - 64 :])
                st = jnp.concatenate([st[: rows - 64], tail], axis=0)
            scores[h, pl.ds(64 * at, rows)] = st
            highest = jnp.maximum(highest, jnp.max(st.reshape(rows // 8, 8, 256), axis=0))
        highest = jnp.max(highest, axis=0, keepdims=True)
        summed = jnp.zeros((8, 256), F32)
        mapped = jnp.zeros((128, 256), F32)
        for at, size in blocks:
            rows = 64 * size
            weights = jnp.exp2((scores[h, pl.ds(64 * at, rows)] - highest) * EXP_SCALE)
            summed = summed + jnp.sum(weights.reshape(rows // 8, 8, 256), axis=0)
            mapped = mapped + jnp.dot(
                vt[:, pl.ds(64 * at, rows)], weights.astype(BF16), preferred_element_type=F32
            )
        mapped = mapped * (1.0 / jnp.sum(summed, axis=0, keepdims=True))
        combined = mapped[:, :128] - lam * mapped[:, 128:]
        mean_sq = jnp.sum(combined * combined, axis=0, keepdims=True) * (1.0 / 128)
        normed = (combined * lax.rsqrt(mean_sq + 1e-5)).T * gain
        ostage[item, pl.ds(first, 2)] = normed.astype(BF16).reshape(2, 64, 128)


def kernel(
    q_hbm, k_hbm, v_hbm, gate_hbm, lam_ref, gain_ref, w_hbm, out_ref,
    src, recv, vt, scores, ostage, orecv, wall, gate, sig, gated,
    load_sem, gate_sem, wload_sem, kv_send, kv_recv, q_recv, o_send, o_recv,
    wz_send, wz_recv, wy_send, wy_recv, wx_send, wx_recv, wp_send, wp_recv,
):
    me = lax.axis_index("sp")
    dp = lax.axis_index("dp")
    z, y = me // NY, lax.rem(me, NY)
    x, core = dp // 2, lax.rem(dp, 2)

    def plane_peer(dz, dy):
        return lax.rem(z + dz, NZ) * NY + lax.rem(y + dy, NY)

    def x_peer(dx):
        return lax.rem(x + dx, NX) * 2 + core

    partner = x * 2 + 1 - core
    barrier = pltpu.get_barrier_semaphore()

    @pl.loop(1, NSP)
    def _(d):
        pl.semaphore_signal(
            barrier, inc=1, device_id=(lax.rem(me + d, NSP), dp), device_id_type=MESH
        )

    @pl.loop(1, NX)
    def _(d):
        pl.semaphore_signal(barrier, inc=1, device_id=(me, x_peer(d)), device_id_type=MESH)

    pl.semaphore_signal(barrier, inc=1, device_id=(me, partner), device_id_type=MESH)

    def local(a, b, sem):
        copy = pltpu.make_async_copy(a, b, sem)
        copy.start()
        return copy

    tensors = (k_hbm, v_hbm, q_hbm)
    w_load = local(w_hbm, wall.at[dp, z, y], wload_sem)
    loads = []
    for i in range(2):
        loads.append(
            [
                local(t.at[pl.ds(NSP * i, NSP)], src.at[pl.ds(NSP * i, NSP), n], load_sem.at[i, n])
                for n, t in enumerate(tensors)
            ]
        )
        for n, t in enumerate(tensors):
            local(
                t.at[NSP * i + me],
                recv.at[i, me, n],
                kv_recv.at[i] if n < 2 else q_recv.at[i, z],
            )
    gate_load = local(gate_hbm, gate, gate_sem)

    w_load.wait()
    pl.semaphore_wait(barrier, NSP - 1 + NX - 1 + 1)

    def remote(a, b, send, rcv, sp, d):
        copy = pltpu.make_async_remote_copy(
            src_ref=a, dst_ref=b, send_sem=send, recv_sem=rcv, device_id=(sp, d), device_id_type=MESH
        )
        copy.start()

    def drain(ref, sem):
        pltpu.make_async_copy(ref, ref, sem).wait()

    @pl.loop(1, NZ)
    def _(d):
        block = wall.at[dp, z, y]
        remote(block, block, wz_send, wz_recv, plane_peer(d, 0), dp)

    def send_inputs(i, start, count, rcv):
        @pl.loop(0, NSP)
        def _(n):
            dz, dy = slab_offset(n // NY), lax.rem(n, NY)

            @pl.when(n > 0)
            def _():
                to = plane_peer(dz, dy)
                remote(
                    src.at[NSP * i + to, pl.ds(start, count)],
                    recv.at[i, me, pl.ds(start, count)],
                    kv_send,
                    rcv,
                    to,
                    dp,
                )

    for i in range(2):
        for copy in loads[i][:2]:
            copy.wait()
        send_inputs(i, 0, 2, kv_recv.at[i])
        loads[i][2].wait()
        send_inputs(i, 2, 1, q_recv.at[i, z])
        if i == 0:
            drain(wall.at[dp, pl.ds(0, NZ - 1), y], wz_recv)
            mine = wall.at[dp, :, y]

            @pl.loop(1, NY)
            def _(d):
                remote(mine, mine, wy_send, wy_recv, plane_peer(0, d), dp)

            @pl.loop(1, NX)
            def _(d):
                remote(mine, mine, wx_send, wx_recv, me, x_peer(d))

    gate_load.wait()
    for b in range(4):
        sig[b] = jax.nn.sigmoid(gate[b].astype(F32))

    lam = lam_ref[lax.rem(me, 16)]
    gain = gain_ref[...]

    @pl.loop(0, 2)
    def _(item):
        drain(recv.at[0, :, pl.ds(0, 2)], kv_recv.at[item])

        @pl.loop(0, NZ)
        def _(b):
            cols = pl.ds(pl.multiple_of(256 * b, 256), 256)
            vt[:, cols] = recv[item, pl.ds(NY * b, NY), 1].reshape(256, 128).T

        @pl.loop(0, NZ)
        def _(step):
            slab = lax.rem(z + NZ - slab_offset(step), NZ)
            drain(recv.at[0, pl.ds(0, NY), 2], q_recv.at[item, slab])
            for s in range(NZ):

                @pl.when(slab == s)
                def _():
                    slab_attention(s, item, recv, vt, scores, ostage, lam, gain)

            @pl.loop(0, NY)
            def _(n):
                to = slab * NY + n

                @pl.when(to == me)
                def _():
                    orecv[NSP * item + me] = ostage[item, me]

                @pl.when(to != me)
                def _():
                    remote(
                        ostage.at[item, to], orecv.at[NSP * item + me], o_send, o_recv.at[item], to, dp
                    )

        @pl.when(item == 0)
        def _():
            drain(wall.at[dp, :, pl.ds(0, NY - 1)], wy_recv)

            @pl.loop(1, NY)
            def _(dy):
                rows = wall.at[dp, :, lax.rem(y + dy, NY)]

                @pl.loop(1, NX)
                def _(d):
                    remote(rows, rows, wx_send, wx_recv, me, x_peer(d))

            remote(wall.at[dp], wall.at[dp], wp_send, wp_recv, me, partner)

    drain(wall.at[pl.ds(0, NX - 1)], wx_recv)

    @pl.loop(1, NX)
    def _(d):
        rows = wall.at[x_peer(d)]
        remote(rows, rows, wp_send, wp_recv, me, partner)

    for i in range(2):
        drain(orecv.at[pl.ds(0, NSP - 1)], o_recv.at[i])

        @pl.loop(0, 16)
        def _(h):
            cols = pl.ds(pl.multiple_of(128 * h, 128), 128)
            for b in (2 * i, 2 * i + 1):
                gated[pl.ds(64 * b, 64), cols] = (
                    sig[b, :, cols] * orecv[16 * b + h].astype(F32)
                ).astype(BF16)

    drain(wall.at[pl.ds(0, NX)], wp_recv)

    @pl.loop(0, NDP)
    def _(c):
        cols = pl.ds(pl.multiple_of(256 * c, 256), 256)
        out_ref[:, cols] = jnp.dot(
            gated[...], wall[c].reshape(2048, 256), preferred_element_type=F32
        ).astype(BF16)

    drain(src.at[pl.ds(0, 2 * (NSP - 1))], kv_send)
    drain(ostage.at[0, pl.ds(0, NSP - 1)], o_send)
    drain(ostage.at[0, pl.ds(0, NSP - 1)], o_send)
    drain(wall.at[dp, pl.ds(0, NZ - 1), y], wz_send)
    drain(wall.at[dp, :, pl.ds(0, NY - 1)], wy_send)
    drain(wall.at[pl.ds(0, NX - 1)], wx_send)
    drain(wall.at[pl.ds(0, NX)], wp_send)


def on_device(queries, key_maps, value_rows, gate_logits, mix_lambda, head_gain, out_weight):
    items = 64
    any_spec = pl.BlockSpec(memory_space=pl.ANY)
    dma = pltpu.SemaphoreType.DMA
    gate_by_seq = jnp.transpose(gate_logits, (1, 0, 2))
    out = pl.pallas_call(
        kernel,
        out_shape=jax.ShapeDtypeStruct((256, 2048), BF16),
        in_specs=[any_spec, any_spec, any_spec, any_spec, pl.BlockSpec(memory_space=pltpu.SMEM),
                  pl.BlockSpec(memory_space=pltpu.VMEM), any_spec],
        out_specs=pl.BlockSpec(memory_space=pltpu.VMEM),
        scratch_shapes=[
            pltpu.VMEM((items, 3, 64, 128), BF16),
            pltpu.VMEM((2, NSP, 3, 64, 128), BF16),
            pltpu.VMEM((128, 2048), BF16),
            pltpu.VMEM((2, 2048, 256), F32),
            pltpu.VMEM((2, NSP, 64, 128), BF16),
            pltpu.VMEM((items, 64, 128), BF16),
            pltpu.VMEM((NDP, NZ, NY, 64, 256), BF16),
            pltpu.VMEM((4, 64, 2048), BF16),
            pltpu.VMEM((4, 64, 2048), F32),
            pltpu.VMEM((256, 2048), BF16),
            dma((2, 3)), dma, dma, dma, dma((2,)), dma((2, NZ)), dma, dma((2,)),
            dma, dma, dma, dma, dma, dma, dma, dma,
        ],
        compiler_params=pltpu.CompilerParams(
            collective_id=0, has_side_effects=True, vmem_limit_bytes=60 << 20
        ),
        name="fused_layer",
    )(
        queries.reshape(items, 64, 128),
        key_maps.reshape(items, 64, 128),
        value_rows.reshape(items, 64, 128),
        gate_by_seq,
        mix_lambda,
        head_gain.reshape(1, 128),
        out_weight,
    )
    return jnp.transpose(out.reshape(4, 64, 2048), (1, 0, 2))


def solution(mesh):
    return jax.shard_map(
        on_device,
        mesh=mesh,
        in_specs=(
            P("dp", None, "sp", None),
            P("dp", None, "sp", None),
            P("dp", None, "sp", None),
            P("sp", "dp", None),
            P(),
            P(),
            P("sp", "dp"),
        ),
        out_specs=P("sp", "dp", None),
        check_vma=False,
    )
```

time: 285 us -> 119 us (0.42)
  Pallas kernels: 0 us -> 113 us
  matrix products: 63.3 us -> 0 us
  waiting for transfers between devices: 62 us -> 0 us
  blocking collectives: 53.5 us -> 0 us
  local copies, waits for them, and re-layouts: 42.6 us -> 5.78 us
  loops' own time: 19.8 us -> 0 us
  other arithmetic: 17.1 us -> 0 us
  between operations: 13.5 us -> 0.01 us
  starting transfers between devices: 11.1 us -> 0 us
    pallas_call x0 -> x1, Pallas kernels: none -> 113 us  [on_device(): pl.pallas_call(kernel, out_shape=jax.ShapeDtypeStruct((256, 2048), BF16),...]
    dot_general x81 -> x0, matrix products: 63.3 us -> none  [the longest x40 43.4 us: update(): jnp.dot(weights.astype(jnp.bfloat16), value_block, preferred_element_type...]
    all_gather x2 -> x0, waiting for transfers between devices: 56.3 us -> none  [the longest x1 56.3 us: gather_axes(): out = lax.all_gather(out, axes[number], axis=dim, tiled=True)]
    all_to_all x1 -> x0, blocking collectives: 35.8 us -> none  [on_device(): lax.all_to_all(shortened(jnp.swapaxes(normed, 0, 1)), SP, split_axis=0, c...]
    another operation x11 -> x0, loops' own time: 19.8 us -> none  [the longest x8 13.5 us: query_block(): carry_state = lax.fori_loop(0, block_index, advance, initial)]
    all_gather x1 -> x0, blocking collectives: 17.7 us -> none  [gather_axes(): out = lax.all_gather(out, axes[number], axis=dim, tiled=True)]
    while x57 -> x0, local copies, waits for them, and re-layouts: 13.2 us -> none
    all_to_all x1 -> x0, starting transfers between devices: 11 us -> none  [side_by_side(): lax.all_to_all(both, axis, split_axis=split_dim, concat_axis=concat_dim,...]
  transfers between devices with their start and end apart: 3 -> 0, of which waited for: 2 -> 0; matrix products, arithmetic and copies ran while one was open for 37% -> 0% of each run, Pallas kernels for 0% -> 0%
where the time goes in v1:
time: 119 us; the launch traced here: 118 us
  Pallas kernels  113 us (95%)
  local copies, waits for them, and re-layouts  5.78 us (5%)
    pallas_call x1, Pallas kernels, on_device(): pl.pallas_call(kernel, out_shape=jax.ShapeDtypeStruct((256, 2048), BF16),...  113 us
    reshape x1, local copies, waits for them, and re-layouts, on_device(): return jnp.transpose(out.reshape(4, 64, 2048), (1, 0, 2))  3.01 us
    unnamed x1, local copies, waits for them, and re-layouts  2.77 us

profile of v1, /device:TPU:64, one launch (start us, length us, event | category | flops | bytes accessed | tf_op | source)
XLA Modules:
  0.0 118.4 jit_solution(4276848147213795198)
XLA Ops:
  0.0 2.8 %copy.13 = bf16[64,4,2048]{2,0,1:T(8,128)(2,1)} copy(bf16[64,4,2048]{2,1,0:T(4,128)(2,1)} %param.10) | data formatting | bytes 2097152 | tf_op args[3]
  2.8 112.6 %fused_layer.1 = bf16[256,2048]{1,0:T(8,128)(2,1)} custom-call(bf16[64,64,128]{2,1,0:T(8,128)(2,1)} %bitcast.13, bf16[64,64,128]{2,1,0:T(8,128)(2,1)} %bitcast.14, bf16[64,64,128]{2,1,0:T(8,128)(2,1)} %bitcast.15, bf16[4,64,2048]{2,1,0:T(8,128)(2,1)} %bitcast.12, f32[16]{0:T(128)} %lam_ref.1, f32[1,128]{1,0:T(1,128)} %bitcast.16, bf16[64,256]{1,0:T(8,128)(2,1)} %w_hbm.1), custom_call_target="tpu_custom_call" | custom-call | tf_op jit(solution)/shard_map/fused_layer/pallas_call | solution.py:272
  115.4 3.0 %copy.12 = bf16[4,64,2048]{2,0,1:T(4,128)(2,1)} copy(bf16[4,64,2048]{2,1,0:T(8,128)(2,1)} %bitcast.11) | data formatting | bytes 2097152 | tf_op jit(solution)/shard_map/reshape | solution.py:305

commit v2 on v1

v2 whole, which is shorter than its diff:
```python
import math

import jax
import jax.numpy as jnp
from jax import lax
from jax.experimental import pallas as pl
from jax.experimental.pallas import tpu as pltpu
from jax.sharding import PartitionSpec as P

MESH = pl.DeviceIdType.MESH
HEAD_DIM = 64
NZ, NY, NX = 8, 4, 4
NSP, NDP = NZ * NY, 2 * NX
AHEAD_1, AHEAD_2 = 8, 14
EXP_SCALE = HEAD_DIM ** (-0.5) * math.log2(math.e)
F32, BF16 = jnp.float32, jnp.bfloat16


def slab_offset(step):
    return step // 2 + 4 * (step % 2)


def transpose_values(kvq, vt, block):
    cols = pl.ds(pl.multiple_of(256 * block, 256), 256)
    vt[:, cols] = kvq[pl.ds(NY * block, NY), 1].reshape(256, 128).T


def slab_attention(s, kvq, vt, scores, out, lam, gain):
    lane = lax.broadcasted_iota(jnp.int32, (128, 128), 1)
    half_lane = lax.rem(lax.broadcasted_iota(jnp.int32, (64, 256), 1), 128)
    for h in range(2):
        first = NY * s + 2 * h
        q = kvq[pl.ds(first, 2), 2].reshape(128, 128)
        zero = jnp.zeros_like(q)
        qm = jnp.concatenate(
            [jnp.where(lane < HEAD_DIM, q, zero), jnp.where(lane >= HEAD_DIM, q, zero)], axis=0
        )
        chunks = first + 2
        blocks = []
        at = 0
        while at < chunks:
            size = min(4, chunks - at)
            blocks.append((at, size))
            at += size
        highest = jnp.full((8, 256), -1e30, F32)
        for at, size in blocks:
            rows = 64 * size
            keys = kvq[pl.ds(at, size), 0].reshape(rows, 128)
            st = lax.dot_general(
                keys, qm, (((1,), (1,)), ((), ())), preferred_element_type=F32
            )
            if at + size == chunks:
                tail = jnp.where(half_lane < 64, -1e30, st[rows - 64 :])
                st = jnp.concatenate([st[: rows - 64], tail], axis=0)
            scores[h, pl.ds(64 * at, rows)] = st
            highest = jnp.maximum(highest, jnp.max(st.reshape(rows // 8, 8, 256), axis=0))
        highest = jnp.max(highest, axis=0, keepdims=True)
        summed = jnp.zeros((8, 256), F32)
        mapped = jnp.zeros((128, 256), F32)
        for at, size in blocks:
            rows = 64 * size
            weights = jnp.exp2((scores[h, pl.ds(64 * at, rows)] - highest) * EXP_SCALE)
            summed = summed + jnp.sum(weights.reshape(rows // 8, 8, 256), axis=0)
            mapped = mapped + jnp.dot(
                vt[:, pl.ds(64 * at, rows)], weights.astype(BF16), preferred_element_type=F32
            )
        mapped = mapped * (1.0 / jnp.sum(summed, axis=0, keepdims=True))
        combined = mapped[:, :128] - lam * mapped[:, 128:]
        mean_sq = jnp.sum(combined * combined, axis=0, keepdims=True) * (1.0 / 128)
        normed = (combined * lax.rsqrt(mean_sq + 1e-5)).T * gain
        out[pl.ds(first, 2)] = normed.astype(BF16).reshape(2, 64, 128)


def kernel(
    q_hbm, k_hbm, v_hbm, gate_hbm, lam_ref, gain_ref, w_hbm, out_ref,
    src, recv, vt, scores, ostage, orecv, wall, gate, mixed, sig, gated, acc,
    load_sem, gate_sem, wload_sem, kv_send, kv_recv, q_send, q_recv, o_send, o_recv,
    wz_send, wz_recv, wy_send, wy_recv, wx_send, wx_recv, wp_send, wp_recv,
):
    me = lax.axis_index("sp")
    dp = lax.axis_index("dp")
    z, y = me // NY, lax.rem(me, NY)
    x, core = dp // 2, lax.rem(dp, 2)

    def plane_peer(dz, dy):
        return lax.rem(z + dz, NZ) * NY + lax.rem(y + dy, NY)

    def x_peer(dx):
        return lax.rem(x + dx, NX) * 2 + core

    partner = x * 2 + 1 - core
    barrier = pltpu.get_barrier_semaphore()

    @pl.loop(1, NSP)
    def _(d):
        pl.semaphore_signal(
            barrier, inc=1, device_id=(lax.rem(me + d, NSP), dp), device_id_type=MESH
        )

    @pl.loop(1, NX)
    def _(d):
        pl.semaphore_signal(barrier, inc=1, device_id=(me, x_peer(d)), device_id_type=MESH)

    pl.semaphore_signal(barrier, inc=1, device_id=(me, partner), device_id_type=MESH)

    def local(a, b, sem):
        copy = pltpu.make_async_copy(a, b, sem)
        copy.start()
        return copy

    def remote(a, b, send, rcv, sp, d):
        copy = pltpu.make_async_remote_copy(
            src_ref=a, dst_ref=b, send_sem=send, recv_sem=rcv, device_id=(sp, d), device_id_type=MESH
        )
        copy.start()

    def drain(ref, sem):
        pltpu.make_async_copy(ref, ref, sem).wait()

    tensors = (k_hbm, v_hbm, q_hbm)
    w_load = local(w_hbm, wall.at[dp, z, y], wload_sem)
    loads = []
    for i in range(2):
        loads.append(
            [local(t.at[i], src.at[i, :, :, n], load_sem.at[i, n]) for n, t in enumerate(tensors)]
        )
        for n, t in enumerate(tensors):
            local(
                t.at[i, z, y],
                recv.at[i, me, n],
                kv_recv.at[i] if n < 2 else q_recv.at[i, z],
            )
    gate_load = local(gate_hbm, gate, gate_sem)

    w_load.wait()
    for i in range(2):
        for copy in loads[i]:
            copy.wait()
    pl.semaphore_wait(barrier, NSP - 1 + NX - 1 + 1)

    def send_weights_z(row, dz, rcv):
        block = wall.at[dp, row, y]
        remote(block, block, wz_send, rcv, plane_peer(dz, 0), dp)

    def send_weights_x(col):
        rows = wall.at[dp, :, col]

        @pl.loop(1, NX)
        def _(d):
            remote(rows, rows, wx_send, wx_recv, me, x_peer(d))

    def send_kv(i, start, stop):
        @pl.loop(start, stop)
        def _(n):
            to = plane_peer(slab_offset(n // NY), lax.rem(n, NY))
            remote(
                src.at[i, to // NY, lax.rem(to, NY), pl.ds(0, 2)],
                recv.at[i, me, pl.ds(0, 2)],
                kv_send,
                kv_recv.at[i],
                to,
                dp,
            )

    def send_q(i):
        @pl.loop(1, NSP)
        def _(n):
            to = plane_peer(slab_offset(n // NY), lax.rem(n, NY))
            remote(
                src.at[i, to // NY, lax.rem(to, NY), 2],
                recv.at[i, me, 2],
                q_send,
                q_recv.at[i, z],
                to,
                dp,
            )

    for dz in (1, NZ - 1, 2, NZ - 2):
        send_weights_z(z, dz, wz_recv.at[0])
    send_kv(0, 1, AHEAD_1)
    drain(wall.at[dp, pl.ds(0, 4), y], wz_recv.at[0])
    before, after = lax.rem(z + NZ - 2, NZ), lax.rem(z + 2, NZ)
    send_weights_z(before, 1, wz_recv.at[1])
    send_weights_z(before, 2, wz_recv.at[1])
    send_weights_z(after, NZ - 1, wz_recv.at[1])
    send_kv(0, AHEAD_1, AHEAD_2)
    drain(wall.at[dp, pl.ds(0, 3), y], wz_recv.at[1])

    @pl.loop(1, NY)
    def _(d):
        mine = wall.at[dp, :, y]
        remote(mine, mine, wy_send, wy_recv, plane_peer(0, d), dp)

    send_weights_x(y)
    send_kv(0, AHEAD_2, NSP)
    send_q(0)

    gate_load.wait()

    @pl.loop(0, 16)
    def _(n):
        rows = pl.ds(pl.multiple_of(4 * n, 4), 4)
        mixed[rows] = jax.nn.sigmoid(gate[rows].astype(F32))

    for b in range(4):
        sig[b] = mixed[:, b]

    drain(wall.at[dp, :, pl.ds(0, NY - 1)], wy_recv)

    @pl.loop(1, NY)
    def _(d):
        send_weights_x(lax.rem(y + d, NY))

    remote(wall.at[dp], wall.at[dp], wp_send, wp_recv, me, partner)
    send_kv(1, 1, NSP)
    send_q(1)

    gain = gain_ref[...]
    lam = lam_ref[lax.rem(me, 16)]

    @pl.loop(0, 2)
    def _(item):
        drain(recv.at[0, :, pl.ds(0, 2)], kv_recv.at[item])
        kvq = recv.at[item]

        @pl.loop(0, NZ)
        def _(b):
            transpose_values(kvq, vt, b)

        @pl.loop(0, NZ)
        def _(step):
            slab = lax.rem(z + NZ - slab_offset(step), NZ)
            drain(recv.at[0, pl.ds(0, NY), 2], q_recv.at[item, slab])
            for s in range(NZ):

                @pl.when(slab == s)
                def _():
                    slab_attention(s, kvq, vt, scores, ostage.at[item], lam, gain)

            @pl.loop(0, NY)
            def _(n):
                to = slab * NY + n

                @pl.when(to == me)
                def _():
                    orecv[item, z, y] = ostage[item, me]

                @pl.when(to != me)
                def _():
                    remote(
                        ostage.at[item, to],
                        orecv.at[item, z, y],
                        o_send,
                        o_recv.at[item, z],
                        to,
                        dp,
                    )

        @pl.when(item == 0)
        def _():
            drain(wall.at[pl.ds(0, NX - 1)], wx_recv)

            @pl.loop(1, NX)
            def _(d):
                rows = wall.at[x_peer(d)]
                remote(rows, rows, wp_send, wp_recv, me, partner)

    drain(wall.at[pl.ds(0, NX)], wp_recv)
    acc[...] = jnp.zeros_like(acc)

    @pl.loop(0, NZ)
    def _(step):
        i = step // 4
        j = lax.rem(z + step, 4)
        for b in range(2):
            rank = j + 4 * b

            @pl.when(rank == z)
            def _():
                drain(orecv.at[0, 0, pl.ds(0, NY - 1)], o_recv.at[i, rank])

            @pl.when(rank != z)
            def _():
                drain(orecv.at[0, 0], o_recv.at[i, rank])

            for h in range(4):
                cols = pl.ds(pl.multiple_of(512 * j + 128 * h, 128), 128)
                gated[pl.ds(64 * b, 64), pl.ds(128 * h, 128)] = (
                    sig[2 * i + b, :, cols] * orecv[i, rank, h].astype(F32)
                ).astype(BF16)
        for c in range(NDP):
            acc[i, :, pl.ds(256 * c, 256)] += jnp.dot(
                gated[...], wall[c, pl.ds(2 * j, 2)].reshape(512, 256), preferred_element_type=F32
            )

    out_ref[...] = acc[...].astype(BF16)

    drain(recv.at[:, pl.ds(0, NSP - 1), pl.ds(0, 2)], kv_send)
    drain(recv.at[:, pl.ds(0, NSP - 1), 2], q_send)
    drain(ostage.at[:, pl.ds(0, NSP - 1)], o_send)
    drain(wall.at[dp, pl.ds(0, NZ - 1), y], wz_send)
    drain(wall.at[dp, :, pl.ds(0, NY - 1)], wy_send)
    drain(wall.at[pl.ds(0, NX - 1)], wx_send)
    drain(wall.at[pl.ds(0, NX)], wp_send)


def on_device(queries, key_maps, value_rows, gate_logits, mix_lambda, head_gain, out_weight):
    any_spec = pl.BlockSpec(memory_space=pl.ANY)
    dma = pltpu.SemaphoreType.DMA
    out = pl.pallas_call(
        kernel,
        out_shape=jax.ShapeDtypeStruct((2, 128, 2048), BF16),
        in_specs=[any_spec, any_spec, any_spec, any_spec, pl.BlockSpec(memory_space=pltpu.SMEM),
                  pl.BlockSpec(memory_space=pltpu.VMEM), any_spec],
        out_specs=pl.BlockSpec(memory_space=pltpu.VMEM),
        scratch_shapes=[
            pltpu.VMEM((2, NZ, NY, 3, 64, 128), BF16),
            pltpu.VMEM((2, NSP, 3, 64, 128), BF16),
            pltpu.VMEM((128, 2048), BF16),
            pltpu.VMEM((2, 2048, 256), F32),
            pltpu.VMEM((2, NSP, 64, 128), BF16),
            pltpu.VMEM((2, NZ, NY, 64, 128), BF16),
            pltpu.VMEM((NDP, NZ, NY, 64, 256), BF16),
            pltpu.VMEM((64, 4, 2048), BF16),
            pltpu.VMEM((64, 4, 2048), F32),
            pltpu.VMEM((4, 64, 2048), F32),
            pltpu.VMEM((128, 512), BF16),
            pltpu.VMEM((2, 128, 2048), F32),
            dma((2, 3)), dma, dma, dma, dma((2,)), dma, dma((2, NZ)), dma, dma((2, NZ)),
            dma, dma((2,)), dma, dma, dma, dma, dma, dma,
        ],
        compiler_params=pltpu.CompilerParams(
            collective_id=0, has_side_effects=True, vmem_limit_bytes=60 << 20
        ),
        name="fused_layer",
    )(
        queries.reshape(2, NZ, NY, 64, 128),
        key_maps.reshape(2, NZ, NY, 64, 128),
        value_rows.reshape(2, NZ, NY, 64, 128),
        gate_logits,
        mix_lambda,
        head_gain.reshape(1, 128),
        out_weight,
    )
    return jnp.transpose(out.reshape(4, 64, 2048), (1, 0, 2))


def solution(mesh):
    return jax.shard_map(
        on_device,
        mesh=mesh,
        in_specs=(
            P("dp", None, "sp", None),
            P("dp", None, "sp", None),
            P("dp", None, "sp", None),
            P("sp", "dp", None),
            P(),
            P(),
            P("sp", "dp"),
        ),
        out_specs=P("sp", "dp", None),
        check_vma=False,
    )
```

time: 119 us -> 112 us (0.941); the launches traced: 118 us -> 110 us
  Pallas kernels: 113 us -> 107 us
  local copies, waits for them, and re-layouts: 5.78 us -> 3.01 us
    pallas_call x1, Pallas kernels: 113 us -> 107 us  [on_device(): pl.pallas_call(kernel, out_shape=jax.ShapeDtypeStruct((2, 128, 2048), BF1...]
    unnamed x1 -> x0, local copies, waits for them, and re-layouts: 2.77 us -> none
where the time goes in v2:
time: 112 us; the launch traced here: 110 us
  Pallas kernels  107 us (96%)
  local copies, waits for them, and re-layouts  3.01 us (3%)
    pallas_call x1, Pallas kernels, on_device(): pl.pallas_call(kernel, out_shape=jax.ShapeDtypeStruct((2, 128, 2048), BF1...  107 us
    reshape x1, local copies, waits for them, and re-layouts, on_device(): return jnp.transpose(out.reshape(4, 64, 2048), (1, 0, 2))  3.01 us

profile of v2, /device:TPU:64, one launch (start us, length us, event | category | flops | bytes accessed | tf_op | source)
XLA Modules:
  0.0 110.1 jit_solution(875605317234561262)
XLA Ops:
  0.0 107.1 %fused_layer.1 = bf16[2,128,2048]{2,1,0:T(8,128)(2,1)} custom-call(bf16[2,8,4,64,128]{4,3,2,1,0:T(8,128)(2,1)} %bitcast.9, bf16[2,8,4,64,128]{4,3,2,1,0:T(8,128)(2,1)} %bitcast.10, bf16[2,8,4,64,128]{4,3,2,1,0:T(8,128)(2,1)} %bitcast.11, bf16[64,4,2048]{2,1,0:T(4,128)(2,1)} %gate_hbm.1, f32[16]{0:T(128)} %lam_ref.1, f32[1,128]{1,0:T(1,128)} %bitcast.12, ...), custom_call_target="tpu_custom_call" | custom-call | tf_op jit(solution)/shard_map/fused_layer/pallas_call | solution.py:310
  107.1 3.0 %copy.10 = bf16[4,64,2048]{2,0,1:T(4,128)(2,1)} copy(bf16[4,64,2048]{2,1,0:T(8,128)(2,1)} %bitcast.8) | data formatting | bytes 2097152 | tf_op jit(solution)/shard_map/reshape | solution.py:345

commit v3 on v2

--- a/solution.py
+++ b/solution.py
@@ -12,6 +12,7 @@
 NZ, NY, NX = 8, 4, 4
 NSP, NDP = NZ * NY, 2 * NX
 AHEAD_1, AHEAD_2 = 8, 14
+LOCAL = 1
 EXP_SCALE = HEAD_DIM ** (-0.5) * math.log2(math.e)
 F32, BF16 = jnp.float32, jnp.bfloat16
 
@@ -73,14 +74,16 @@
 
 def kernel(
     q_hbm, k_hbm, v_hbm, gate_hbm, lam_ref, gain_ref, w_hbm, out_ref,
-    src, recv, vt, scores, ostage, orecv, wall, gate, mixed, sig, gated, acc,
-    load_sem, gate_sem, wload_sem, kv_send, kv_recv, q_send, q_recv, o_send, o_recv,
+    src, recv, local_in, vt, scores, ostage, local_out, orecv, wall, gate, mixed, sig, gated, acc,
+    load_sem, gate_sem, wload_sem, kv_send, kv_recv, q_send, q_recv, o_send, o_recv, l_send, l_recv, lo_send,
     wz_send, wz_recv, wy_send, wy_recv, wx_send, wx_recv, wp_send, wp_recv,
 ):
     me = lax.axis_index("sp")
     dp = lax.axis_index("dp")
     z, y = me // NY, lax.rem(me, NY)
     x, core = dp // 2, lax.rem(dp, 2)
+    first_slab = z == 0
+    later_slab = z > 0
 
     def plane_peer(dz, dy):
         return lax.rem(z + dz, NZ) * NY + lax.rem(y + dy, NY)
@@ -130,6 +133,12 @@
                 recv.at[i, me, n],
                 kv_recv.at[i] if n < 2 else q_recv.at[i, z],
             )
+    @pl.when(first_slab)
+    def _():
+        for i in range(LOCAL):
+            for n, t in enumerate(tensors):
+                local(t.at[i, pl.ds(1, NZ - 1), y], local_in.at[i, :, y, n], l_recv.at[i])
+
     gate_load = local(gate_hbm, gate, gate_sem)
 
     w_load.wait()
@@ -152,7 +161,8 @@
     def send_kv(i, start, stop):
         @pl.loop(start, stop)
         def _(n):
-            to = plane_peer(slab_offset(n // NY), lax.rem(n, NY))
+            spot = lax.rem(5 * n, NSP)
+            to = plane_peer(spot // NY, lax.rem(spot, NY))
             remote(
                 src.at[i, to // NY, lax.rem(to, NY), pl.ds(0, 2)],
                 recv.at[i, me, pl.ds(0, 2)],
@@ -163,7 +173,7 @@
             )
 
     def send_q(i):
-        @pl.loop(1, NSP)
+        @pl.loop(1, jnp.where(first_slab, NY, NSP) if i < LOCAL else NSP)
         def _(n):
             to = plane_peer(slab_offset(n // NY), lax.rem(n, NY))
             remote(
@@ -174,6 +184,21 @@
                 to,
                 dp,
             )
+
+    def send_local(i):
+        @pl.when(first_slab)
+        def _():
+            @pl.loop(1, NY)
+            def _(d):
+                to = lax.rem(y + d, NY)
+                remote(
+                    src.at[i, pl.ds(1, NZ - 1), to],
+                    local_in.at[i, :, y],
+                    l_send,
+                    l_recv.at[i],
+                    to,
+                    dp,
+                )
 
     for dz in (1, NZ - 1, 2, NZ - 2):
         send_weights_z(z, dz, wz_recv.at[0])
@@ -194,6 +219,7 @@
     send_weights_x(y)
     send_kv(0, AHEAD_2, NSP)
     send_q(0)
+    send_local(0)
 
     gate_load.wait()
 
@@ -230,40 +256,70 @@
         @pl.loop(0, NZ)
         def _(step):
             slab = lax.rem(z + NZ - slab_offset(step), NZ)
-            drain(recv.at[0, pl.ds(0, NY), 2], q_recv.at[item, slab])
-            for s in range(NZ):
-
-                @pl.when(slab == s)
-                def _():
-                    slab_attention(s, kvq, vt, scores, ostage.at[item], lam, gain)
-
-            @pl.loop(0, NY)
-            def _(n):
-                to = slab * NY + n
-
-                @pl.when(to == me)
-                def _():
-                    orecv[item, z, y] = ostage[item, me]
-
-                @pl.when(to != me)
-                def _():
+            here = jnp.logical_or(first_slab, slab > 0)
+
+            @pl.when(jnp.logical_or(here, item >= LOCAL))
+            def _():
+                drain(recv.at[0, pl.ds(0, NY), 2], q_recv.at[item, slab])
+                for s in range(NZ):
+
+                    @pl.when(slab == s)
+                    def _():
+                        slab_attention(s, kvq, vt, scores, ostage.at[item], lam, gain)
+
+                @pl.loop(0, NY)
+                def _(n):
+                    to = slab * NY + n
+
+                    @pl.when(to == me)
+                    def _():
+                        orecv[item, z, y] = ostage[item, me]
+
+                    @pl.when(to != me)
+                    def _():
+                        remote(
+                            ostage.at[item, to],
+                            orecv.at[item, z, y],
+                            o_send,
+                            o_recv.at[item, z],
+                            to,
+                            dp,
+                        )
+
+            @pl.when(jnp.logical_and(item == 1, step == 2))
+            def _():
+                drain(wall.at[pl.ds(0, NX - 1)], wx_recv)
+
+                @pl.loop(1, NX)
+                def _(d):
+                    rows = wall.at[x_peer(d)]
+                    remote(rows, rows, wp_send, wp_recv, me, partner)
+
+        @pl.when(jnp.logical_and(first_slab, item == 0))
+        def _():
+            @pl.loop(0, LOCAL)
+            def _(i):
+                drain(local_in.at[0], l_recv.at[i])
+
+                @pl.loop(0, NZ - 1)
+                def _(j):
+                    block = local_in.at[i, j]
+                    transpose_values(block, vt, 0)
+                    lam_j = lam_ref[lax.rem(NY * (j + 1) + y, 16)]
+                    slab_attention(0, block, vt, scores, local_out.at[i, j], lam_j, gain)
+                    orecv[i, j + 1, y] = local_out[i, j, y]
+
+                @pl.loop(1, NY)
+                def _(d):
+                    to = lax.rem(y + d, NY)
                     remote(
-                        ostage.at[item, to],
-                        orecv.at[item, z, y],
-                        o_send,
-                        o_recv.at[item, z],
+                        local_out.at[i, :, to],
+                        orecv.at[i, pl.ds(1, NZ - 1), y],
+                        lo_send,
+                        o_recv.at[i, z],
                         to,
                         dp,
                     )
-
-        @pl.when(item == 0)
-        def _():
-            drain(wall.at[pl.ds(0, NX - 1)], wx_recv)
-
-            @pl.loop(1, NX)
-            def _(d):
-                rows = wall.at[x_peer(d)]
-                remote(rows, rows, wp_send, wp_recv, me, partner)
 
     drain(wall.at[pl.ds(0, NX)], wp_recv)
     acc[...] = jnp.zeros_like(acc)
@@ -272,14 +328,20 @@
     def _(step):
         i = step // 4
         j = lax.rem(z + step, 4)
+        near = jnp.logical_and(first_slab, i < LOCAL)
+        far = jnp.logical_or(later_slab, i >= LOCAL)
         for b in range(2):
             rank = j + 4 * b
 
-            @pl.when(rank == z)
+            @pl.when(jnp.logical_and(near, rank == 0))
+            def _():
+                drain(orecv.at[0, :, pl.ds(0, NY - 1)], o_recv.at[i, rank])
+
+            @pl.when(jnp.logical_and(far, rank == z))
             def _():
                 drain(orecv.at[0, 0, pl.ds(0, NY - 1)], o_recv.at[i, rank])
 
-            @pl.when(rank != z)
+            @pl.when(jnp.logical_and(far, rank != z))
             def _():
                 drain(orecv.at[0, 0], o_recv.at[i, rank])
 
@@ -296,8 +358,21 @@
     out_ref[...] = acc[...].astype(BF16)
 
     drain(recv.at[:, pl.ds(0, NSP - 1), pl.ds(0, 2)], kv_send)
-    drain(recv.at[:, pl.ds(0, NSP - 1), 2], q_send)
-    drain(ostage.at[:, pl.ds(0, NSP - 1)], o_send)
+    for i in range(2):
+
+        @pl.when(first_slab)
+        def _():
+            drain(recv.at[0, pl.ds(0, NY - 1 if i < LOCAL else NSP - 1), 2], q_send)
+            drain(ostage.at[0, pl.ds(0, NSP - 1)], o_send)
+            if i < LOCAL:
+                drain(local_in.at[0, :, pl.ds(0, NY - 1)], l_send)
+                drain(local_out.at[0, :, pl.ds(0, NY - 1)], lo_send)
+
+        @pl.when(later_slab)
+        def _():
+            drain(recv.at[0, pl.ds(0, NSP - 1), 2], q_send)
+            drain(ostage.at[0, pl.ds(0, NSP - 1 - (NY if i < LOCAL else 0))], o_send)
+
     drain(wall.at[dp, pl.ds(0, NZ - 1), y], wz_send)
     drain(wall.at[dp, :, pl.ds(0, NY - 1)], wy_send)
     drain(wall.at[pl.ds(0, NX - 1)], wx_send)
@@ -316,9 +391,11 @@
         scratch_shapes=[
             pltpu.VMEM((2, NZ, NY, 3, 64, 128), BF16),
             pltpu.VMEM((2, NSP, 3, 64, 128), BF16),
+            pltpu.VMEM((LOCAL, NZ - 1, NY, 3, 64, 128), BF16),
             pltpu.VMEM((128, 2048), BF16),
             pltpu.VMEM((2, 2048, 256), F32),
             pltpu.VMEM((2, NSP, 64, 128), BF16),
+            pltpu.VMEM((LOCAL, NZ - 1, NY, 64, 128), BF16),
             pltpu.VMEM((2, NZ, NY, 64, 128), BF16),
             pltpu.VMEM((NDP, NZ, NY, 64, 256), BF16),
             pltpu.VMEM((64, 4, 2048), BF16),
@@ -326,7 +403,7 @@
             pltpu.VMEM((4, 64, 2048), F32),
             pltpu.VMEM((128, 512), BF16),
             pltpu.VMEM((2, 128, 2048), F32),
-            dma((2, 3)), dma, dma, dma, dma((2,)), dma, dma((2, NZ)), dma, dma((2, NZ)),
+            dma((2, 3)), dma, dma, dma, dma((2,)), dma, dma((2, NZ)), dma, dma((2, NZ)), dma, dma((LOCAL,)), dma,
             dma, dma((2,)), dma, dma, dma, dma, dma, dma,
         ],
         compiler_params=pltpu.CompilerParams(

time: 112 us -> 109 us (0.973); the launches traced: 110 us -> 109 us
  no operation moved by 1% of the time
where the time goes in v3:
time: 109 us
  Pallas kernels  106 us (97%)
  local copies, waits for them, and re-layouts  3.01 us (3%)
    pallas_call x1, Pallas kernels, on_device(): pl.pallas_call(kernel, out_shape=jax.ShapeDtypeStruct((2, 128, 2048), BF1...  106 us
    reshape x1, local copies, waits for them, and re-layouts, on_device(): return jnp.transpose(out.reshape(4, 64, 2048), (1, 0, 2))  3.01 us

profile of v3, /device:TPU:64, one launch (start us, length us, event | category | flops | bytes accessed | tf_op | source)
XLA Modules:
  0.0 109.4 jit_solution(8044095267067538005)
XLA Ops:
  0.0 106.3 %fused_layer.1 = bf16[2,128,2048]{2,1,0:T(8,128)(2,1)} custom-call(bf16[2,8,4,64,128]{4,3,2,1,0:T(8,128)(2,1)} %bitcast.9, bf16[2,8,4,64,128]{4,3,2,1,0:T(8,128)(2,1)} %bitcast.10, bf16[2,8,4,64,128]{4,3,2,1,0:T(8,128)(2,1)} %bitcast.11, bf16[64,4,2048]{2,1,0:T(4,128)(2,1)} %gate_hbm.1, f32[16]{0:T(128)} %lam_ref.1, f32[1,128]{1,0:T(1,128)} %bitcast.12, ...), custom_call_target="tpu_custom_call" | custom-call | tf_op jit(solution)/shard_map/fused_layer/pallas_call | solution.py:385
  106.3 3.0 %copy.10 = bf16[4,64,2048]{2,0,1:T(4,128)(2,1)} copy(bf16[4,64,2048]{2,1,0:T(8,128)(2,1)} %bitcast.8) | data formatting | bytes 2097152 | tf_op jit(solution)/shard_map/reshape | solution.py:422

commit v4 on v3

--- a/solution.py
+++ b/solution.py
@@ -286,7 +286,7 @@
                             dp,
                         )
 
-            @pl.when(jnp.logical_and(item == 1, step == 2))
+            @pl.when(jnp.logical_and(item == 1, step == 4))
             def _():
                 drain(wall.at[pl.ds(0, NX - 1)], wx_recv)
 

time: 109 us -> 109 us (level)
  no operation moved by 1% of the time
where the time goes in v4:
time: 109 us
  Pallas kernels  106 us (97%)
  local copies, waits for them, and re-layouts  3.01 us (3%)
    pallas_call x1, Pallas kernels, on_device(): pl.pallas_call(kernel, out_shape=jax.ShapeDtypeStruct((2, 128, 2048), BF1...  106 us
    reshape x1, local copies, waits for them, and re-layouts, on_device(): return jnp.transpose(out.reshape(4, 64, 2048), (1, 0, 2))  3.01 us

profile of v4, /device:TPU:64, one launch (start us, length us, event | category | flops | bytes accessed | tf_op | source)
XLA Modules:
  0.0 109.4 jit_solution(3453831254584263045)
XLA Ops:
  0.0 106.3 %fused_layer.1 = bf16[2,128,2048]{2,1,0:T(8,128)(2,1)} custom-call(bf16[2,8,4,64,128]{4,3,2,1,0:T(8,128)(2,1)} %bitcast.9, bf16[2,8,4,64,128]{4,3,2,1,0:T(8,128)(2,1)} %bitcast.10, bf16[2,8,4,64,128]{4,3,2,1,0:T(8,128)(2,1)} %bitcast.11, bf16[64,4,2048]{2,1,0:T(4,128)(2,1)} %gate_hbm.1, f32[16]{0:T(128)} %lam_ref.1, f32[1,128]{1,0:T(1,128)} %bitcast.12, ...), custom_call_target="tpu_custom_call" | custom-call | tf_op jit(solution)/shard_map/fused_layer/pallas_call | solution.py:385
  106.3 3.0 %copy.10 = bf16[4,64,2048]{2,0,1:T(4,128)(2,1)} copy(bf16[4,64,2048]{2,1,0:T(8,128)(2,1)} %bitcast.8) | data formatting | bytes 2097152 | tf_op jit(solution)/shard_map/reshape | solution.py:422
